TPU v7x, 128 devices: a whole 4x4x4 slice. The times are simulated.
128 devices in a mesh: fs: 16 (over z, x), tp: 8 (over y, core).
Axes of the slice: x: 4, y: 4, z: 4, core: 2. Of those that a mesh axis runs over, the one named last changes fastest.
Arguments:
- saved_input: bfloat16 [49152, 2048], P('fs'), may hold values from -6 to 6
- proj_cot: bfloat16 [3, 49152, 2048], P(None, 'fs', 'tp'), may hold values from -0.02734375 to 0.02734375
- log_cache: float32 [16, 49152], P(None, 'fs'), as said below
- cache_cot: float32 [16, 49152], P(None, 'fs'), may hold values from -0.02734375 to 0.02734375
- proj_master: float32 [3, 2048, 2048], P(None, 'fs', 'tp'), may hold values from -0.125 to 0.125
- factors: bfloat16 [3, 2048, 256], P(None, 'fs'), may hold values from -0.125 to 0.125
- first_moment: float32 [3, 256, 2048], P(None, None, 'tp'), may hold values from -6 to 6
- second_moment: float32 [3, 256, 2048], P(None, None, 'tp'), may hold values from 0.01 to 10
- gate_master: float32 [16, 2048], replicated, may hold values from -0.125 to 0.125
- gate_first: float32 [16, 2048], replicated, may hold values from -6 to 6
- gate_second: float32 [16, 2048], replicated, may hold values from 0.1 to 3
Outputs:
- proj_step: float32 [3, 2048, 2048], P(None, 'fs', 'tp')
- proj_new: float32 [3, 2048, 2048], P(None, 'fs', 'tp')
- proj_copy: bfloat16 [3, 2048, 2048], P(None, None, 'tp')
- first_new: float32 [3, 256, 2048], P(None, None, 'tp')
- second_new: float32 [3, 256, 2048], P(None, None, 'tp')
- gate_new: float32 [16, 2048], replicated
- gate_copy: bfloat16 [16, 2048], replicated
- gate_first_new: float32 [16, 2048], replicated
- gate_second_new: float32 [16, 2048], replicated
Inputs may be any that keep to these rules, and one draw needn't show every extreme that they name: `log_cache`: each head's values never rise along positions.
All inputs are finite; a program needn't handle non-finite values.
Results may differ from a plain program's by a relative error of at most 0.0004.
Values may be sent and summed in bfloat16 or wider, within the bound.
No kernel may reach another device: no remote copies, remote signals or barrier semaphores. Data moves between devices by JAX's collectives and lax.ppermute only.
A program may use at most 128 MiB of HBM per device.

v0:
```python
import jax
import jax.numpy as jnp
from jax import lax
from jax.sharding import PartitionSpec as P

BETA_ONE = 0.8
BETA_TWO = 0.9
LEARN = 0.001


def from_behind(x, axis, by):
    peers = lax.axis_size(axis)
    pairs = [(i, i + by) for i in range(peers) if 0 <= i + by < peers]
    return lax.ppermute(x, axis, pairs)


def from_everyone(x, axis):
    copies = jnp.broadcast_to(x, (lax.axis_size(axis), *x.shape))
    return lax.all_to_all(copies, axis, split_axis=0, concat_axis=0, tiled=True)


def folded_in_pairs(pieces, combine):
    while len(jax.tree.leaves(pieces)[0]) > 1:
        pieces = jax.vmap(combine)(*(pieces[side::2] for side in (0, 1)))
    return pieces[0]


def carried_in(x, axis, combine, identity):
    peers, place = (lax.axis_size(axis), lax.axis_index(axis))
    passed = jnp.arange(peers) > place

    def kept(part, zero, own):
        part = jnp.where(
            passed.reshape(-1, *(1 for _ in own.shape)), part, jnp.asarray(zero, own.dtype)
        )
        return part[::-1]

    pieces = from_everyone(x, axis)
    return folded_in_pairs(kept(pieces, identity, x), combine)


def rows_for(lines, peers):
    spare = -lines.shape[0] % peers
    if not spare:
        return lines
    return jnp.concatenate([lines, jnp.zeros((spare, *lines.shape[1:]), lines.dtype)])


def in_order(parts, dim):
    parts = jnp.moveaxis(parts, 0, dim)
    lengths = parts.shape
    return parts.reshape(*lengths[:dim], lengths[dim] * lengths[dim + 1], *lengths[dim + 2 :])


def collect(x, axis, dim):
    return in_order(from_everyone(x, axis), dim)


def cut_along(x, dim, peers):
    lengths = x.shape
    parts = x.reshape(*lengths[:dim], peers, lengths[dim] // peers, *lengths[dim + 1 :])
    return jnp.moveaxis(parts, dim, 0)


def summed_on_arrival(x, axis, dim):
    parts = cut_along(x, dim, lax.axis_size(axis))
    arrived = lax.all_to_all(parts, axis, split_axis=0, concat_axis=0, tiled=True)
    return arrived.sum(axis=0)


def total_of(x, axes):
    padded = rows_for(x, lax.axis_size(axes))
    whole = collect(summed_on_arrival(padded, axes, 0), axes, 0)
    return lax.slice_in_dim(whole, 0, len(x)).reshape(x.shape)


def in_one(arrays, axis):
    ravelled, at, finished = (jnp.concatenate([a.reshape(-1) for a in arrays]), 0, [])
    so_far = total_of(ravelled, axis)
    for a in arrays:
        finished.append(so_far[at : at + a.size].reshape(a.shape))
        at += a.size
    return tuple(finished)


def over_copies(x, axis):
    everything = from_everyone(x, axis)
    return jnp.sum(everything, axis=0)


def add_pair(earlier, later_part):
    return earlier + later_part


def local(
    saved_input,
    proj_cot,
    log_cache,
    cache_cot,
    proj_master,
    factors,
    first_moment,
    second_moment,
    gate_master,
    gate_first,
    gate_second,
):
    heads = log_cache.shape[0]
    edge = from_behind(log_cache[:, -1:], "fs", 1)
    previous = jnp.concatenate([edge, log_cache[:, :-1]], axis=1)
    gate_logarithm = log_cache - previous
    carried = carried_in(
        jnp.sum(cache_cot, axis=1), "fs", add_pair, jnp.zeros((heads,), jnp.float32)
    )
    later = jnp.flip(jnp.cumsum(jnp.flip(cache_cot, 1), axis=1), 1) + carried[:, None]
    gate_cot = (later * -jnp.expm1(gate_logarithm)).astype(jnp.bfloat16)
    gate_part = jnp.dot(gate_cot, saved_input, preferred_element_type=jnp.float32)
    all_factors = lax.all_gather(factors, "fs", axis=1, tiled=True)
    reduced = jnp.einsum(
        "td,rdk->rtk", saved_input, all_factors, preferred_element_type=jnp.float32
    )
    upper_half = lax.optimization_barrier(reduced.astype(jnp.bfloat16))
    lower_half = (reduced - upper_half.astype(jnp.float32)).astype(jnp.bfloat16)
    low_part = jnp.einsum("rtk,rtw->rkw", upper_half, proj_cot, preferred_element_type=jnp.float32)
    low_part = low_part + jnp.einsum(
        "rtk,rtw->rkw", lower_half, proj_cot, preferred_element_type=jnp.float32
    )
    low, gate_grad = in_one((low_part, gate_part), "fs")
    first_new = BETA_ONE * first_moment + (1.0 - BETA_ONE) * low
    second_new = BETA_TWO * second_moment + (1.0 - BETA_TWO) * low * low
    direction = first_new / jnp.sqrt(second_new)
    squares = over_copies(jnp.sum(direction * direction), "tp")
    entries = direction.shape[0] * direction.shape[1] * direction.shape[2] * lax.axis_size("tp")
    scale = lax.rsqrt(squares / entries + 1e-06)
    product = jnp.einsum(
        "rdk,rkw->rdw", factors.astype(jnp.float32), direction, precision=lax.Precision.HIGHEST
    )
    proj_step = scale * product
    proj_new = proj_master - LEARN * proj_step
    proj_copy = lax.all_gather(proj_new.astype(jnp.bfloat16), "fs", axis=1, tiled=True)
    gate_first_new = BETA_ONE * gate_first + (1.0 - BETA_ONE) * gate_grad
    gate_second_new = BETA_TWO * gate_second + (1.0 - BETA_TWO) * gate_grad * gate_grad
    gate_new = gate_master - LEARN * gate_first_new / jnp.sqrt(gate_second_new)
    gate_copy = gate_new.astype(jnp.bfloat16)
    return (
        proj_step,
        proj_new,
        proj_copy,
        first_new,
        second_new,
        gate_new,
        gate_copy,
        gate_first_new,
        gate_second_new,
    )


def solution(mesh):
    placed = (
        P("fs", None),
        P(None, "fs", "tp"),
        P(None, "fs"),
        P(None, "fs"),
        P(None, "fs", "tp"),
        P(None, "fs", None),
        P(None, None, "tp"),
        P(None, None, "tp"),
        P(),
        P(),
        P(),
    )
    return jax.shard_map(
        local,
        mesh=mesh,
        in_specs=placed,
        out_specs=(
            P(None, "fs", "tp"),
            P(None, "fs", "tp"),
            P(None, None, "tp"),
            P(None, None, "tp"),
            P(None, None, "tp"),
            P(),
            P(),
            P(),
            P(),
        ),
        check_vma=False,
    )
```

profile of v0, /device:TPU:0, one launch (start us, length us, event | category | flops | bytes accessed | tf_op | source)
XLA Modules:
  0.0 206.4 jit_solution(16304343146461172091)
XLA Ops:
  7.2 0.0 all-gather.3.cloned.1.call-start
  7.2 1.7 copy.44
  9.0 0.0 all-gather.3.cloned.1.call-update
  9.0 1.1 reduce_sum.36
  10.1 0.6 broadcast_in_dim.22
  10.7 8.0 %all-to-all-start = ((f32[16,1,16]{2,1,0:T(1,128)}), f32[16,1,16]{2,1,0:T(1,128)S(1)}, u32[]{:S(2)}, u32[]{:S(2)}) async-start(f32[16,1,16]{2,1,0:T(1,128)} %broadcast_in_dim.22), calls=%async_computation | async-start | bytes 16384 | tf_op jit(solution)/shard_map/all_to_all | solution.py:19
  18.7 0.8 slice.65
  19.4 3.8 %collective-permute-start = (f32[16,1]{1,0:T(8,128)S(1)}, f32[16,1]{1,0:T(8,128)S(1)}, u32[]{:S(2)}, u32[]{:S(2)}) collective-permute-start(f32[16,1]{1,0:T(8,128)S(1)} %slice.65), channel_id=1, source_target_pairs={{0,8},{8,16},{16,24},{24,32},{32,40},{40,48},{48,56},{56,64},{64,7... | collective-permute-start | bytes 200 | tf_op jit(solution)/shard_map/ppermute | solution.py:14
  23.3 9.3 %rev.8 = f32[16,3072]{1,0:T(8,128)S(1)} reverse(f32[16,3072]{1,0:T(8,128)} %param.14), dimensions={1} | reverse | bytes 393216 | tf_op jit(solution)/shard_map/jit(_flip)/rev | solution.py:115
  32.6 4.6 %reduce-window.6 = f32[16,24,128]{2,1,0:T(8,128)S(1)} reduce-window(f32[16,24,128]{2,1,0:T(8,128)S(1)} %bitcast.46, f32[]{:T(128)} %constant.11.clone.1), window={size=1x1x128 pad=0_0x0_0x127_0}, to_apply=%region_0.0 | reduce-window | flops 6242304 | bytes 393220 | tf_op jit(solution)/shard_map/reduce-window
  37.3 0.2 slice_reduce_fusion
  37.5 0.2 reduce-window.9
  37.7 0.1 broadcast_add_fusion
  37.8 1.8 rev.9
  39.6 0.0 all-to-all-done
  39.6 0.1 broadcast_select_fusion
  39.9 0.0 collective-permute-done
  39.9 6.6 %convolution_bitcast_fusion = f32[2,16,8,128]{3,2,1,0:T(8,128)S(1)} fusion(bf16[3072,2048]{1,0:T(8,128)(2,1)} %param.11, f32[16,3072]{1,0:T(8,128)} %param.13, f32[16,3071]{1,0:T(8,128)} %bitcast.43, f32[16,1]{1,0:T(8,128)S(1)} %collective-permute-done, f32[16,3072]{1,0:T(8,128)S(1)} %rev.9, f32[16]{0:T(128)S(1)} %add_bitcast_fusion), kind=kOutput, calls=%fused_computation.10 | convolution fusion | flops 201621504 | bytes 13303872 | tf_op jit(solution)/shard_map/dot_general | solution.py:117
  46.5 18.7 %all-gather.3.cloned.1.call-done = bf16[3,2048,256]{1,2,0:T(8,128)(2,1)} async-done(((bf16[3,128,256]{1,2,0:T(8,128)(2,1)}), bf16[3,2048,256]{1,2,0:T(8,128)(2,1)}) %all-gather.3.cloned.1.call-update) | async-done | bytes 3145744 | tf_op jit(solution)/shard_map/all_gather | solution.py:118
  65.3 16.1 %bitcast_convert_fusion = (bf16[3,3072,256]{1,2,0:T(8,128)(2,1)S(1)}, f32[3,256,3072]{2,1,0:T(8,128)}) fusion(bf16[3,2048,256]{1,2,0:T(8,128)(2,1)} %all-gather.3.cloned.1.call-done, bf16[3072,2048]{1,0:T(8,128)(2,1)} %param.11), kind=kOutput, calls=%fused_computation.3 | convolution fusion | flops 9666035712 | bytes 29884416 | tf_op jit(solution)/shard_map/td,rdk->rtk/dot_general | solution.py:119
  81.4 3.7 %fusion.22 = f32[3,256,256]{2,1,0:T(8,128)S(1)} fusion(bf16[3,3072,256]{1,2,0:T(8,128)(2,1)S(1)} %get-tuple-element.63, bf16[3,3072,256]{2,1,0:T(8,128)(2,1)} %param.12), kind=kOutput, calls=%fused_computation.36 | convolution fusion | flops 1207959552 | bytes 10223616 | tf_op jit(solution)/shard_map/rtk,rtw->rkw/dot_general | solution.py:124
  85.1 6.4 %fusion.5 = f32[3,256,256]{2,1,0:T(8,128)S(1)} fusion(f32[3,256,256]{2,1,0:T(8,128)S(1)} %fusion.22, bf16[3,3072,256]{2,1,0:T(8,128)(2,1)} %param.12, f32[3,256,3072]{2,1,0:T(8,128)} %get-tuple-element.64, bf16[3,3072,256]{1,2,0:T(8,128)(2,1)S(1)} %get-tuple-element.63), kind=kOutput, calls=%fused_computation.6 | convolution fusion | flops 1215234048 | bytes 20447232 | tf_op jit(solution)/shard_map/rtk,rtw->rkw/dot_general | solution.py:125
  91.5 0.0 copy-start.3
  91.5 0.4 copy.55
  91.9 0.1 pad_maximum_fusion
  92.0 19.2 %all_to_all.30 = f32[16,1,14336]{2,1,0:T(1,128)S(1)} all-to-all(f32[16,1,14336]{2,1,0:T(1,128)S(1)} %bitcast.40), channel_id=1, replica_groups=mesh['fs'=16,'tp'=8] {'fs'}, dimensions={0} | all-to-all | bytes 1835008 | tf_op jit(solution)/shard_map/all_to_all | solution.py:67
  111.2 0.6 reduce_sum.37
  111.8 1.4 broadcast_in_dim.24
  113.2 0.0 copy-start.2
  113.2 3.8 %all-to-all-start.2 = ((f32[16,1,14336]{2,1,0:T(1,128)}), f32[16,1,14336]{2,1,0:T(1,128)S(1)}, u32[]{:S(2)}, u32[]{:S(2)}) async-start(f32[16,1,14336]{2,1,0:T(1,128)} %broadcast_in_dim.24), calls=%async_computation.2 | async-start | bytes 1835008 | tf_op jit(solution)/shard_map/all_to_all | solution.py:19
  117.0 0.2 all-gather.5.cloned.1.call-start
  117.2 0.0 copy-done.3
  117.2 0.9 copy.48
  118.1 12.4 %all-to-all-done.2 = f32[16,1,14336]{2,1,0:T(1,128)S(1)} async-done(((f32[16,1,14336]{2,1,0:T(1,128)}), f32[16,1,14336]{2,1,0:T(1,128)S(1)}, u32[]{:S(2)}, u32[]{:S(2)}) %all-to-all-start.2) | async-done | bytes 917536 | tf_op jit(solution)/shard_map/all_to_all | solution.py:19
  130.5 0.1 slice.72
  130.6 0.2 reshape.69
  130.8 2.3 %multiply_reduce_fusion = (f32[]{:T(128)}, f32[3,256,256]{2,1,0:T(8,128)S(1)}, f32[3,256,256]{2,1,0:T(8,128)S(1)}) fusion(f32[3,256,256]{2,1,0:T(8,128)S(1)} %reshape.69, f32[3,256,256]{2,1,0:T(8,128)} %param.18, f32[3,256,256]{2,1,0:T(8,128)} %param.17), kind=kLoop, calls=%fused_computation.13 | loop fusion | flops 1966079 | bytes 3932164 | tf_op jit(solution)/shard_map/reduce_sum | solution.py:132
  133.1 0.0 copy-start.1
  133.1 0.0 copy-start
  133.1 0.0 copy-start.4
  133.1 0.0 copy-start.5
  133.1 0.7 broadcast_in_dim.25
  133.8 9.4 %all_to_all.31 = f32[8,1,1]{2,1,0:T(1,128)S(1)} all-to-all(f32[8,1,1]{2,1,0:T(1,128)S(1)} %broadcast_in_dim.25), channel_id=1, replica_groups=mesh['fs'=16,'tp'=8] {'tp'}, dimensions={0} | all-to-all | bytes 64 | tf_op jit(solution)/shard_map/all_to_all | solution.py:19
  143.2 0.6 reduce_sum.39
  144.5 0.0 copy-done.2
  144.5 2.7 %fusion.20 = (bf16[3,128,256]{1,2,0:T(8,128)(2,1)}, f32[3,128,256]{1,2,0:T(8,128)S(1)}, f32[3,128,256]{1,2,0:T(8,128)}) fusion(f32[3,128,256]{1,2,0:T(8,128)} %copy.48, bf16[3,128,256]{2,1,0:T(8,128)(2,1)S(1)} %copy-done.2, f32[3,256,256]{2,1,0:T(8,128)S(1)} %get-tuple-element.62, f32[3,256,256]{2,1,0:T(8,128)S(1)} %get-tuple-element.61, f32[]{:T(128)S(6)} %rsqrt.5), kind=kOutput, calls=%fused_computation.35 | convolution fusion | flops 302579712 | bytes 3145732 | tf_op jit(solution)/shard_map/rdk,rkw->rdw/dot_general | solution.py:135
  147.1 0.0 copy-done.1
  147.1 0.0 all-gather.5.cloned.1.call-update
  147.2 2.2 %reduce.3 = f32[16,14336]{1,0:T(8,128)S(1)} reduce(f32[16,1,14336]{2,1,0:T(1,128)S(1)} %all-to-all-done.2, f32[]{:T(128)} %constant.8), dimensions={1}, to_apply=%all_to_all.24.reduce_sub_computation | reduce | bytes 1835012 | tf_op jit(solution)/shard_map/all_to_all | solution.py:19
  149.4 0.1 slice.68
  149.5 0.0 copy-done.4
  149.5 0.0 copy-done.5
  149.5 1.7 fusion.18
  151.2 1.9 copy.49
  153.1 0.9 copy.50
  154.1 0.0 copy-done
  154.1 40.8 %all-gather.5.cloned.1.call-done = bf16[3,2048,256]{1,2,0:T(8,128)(2,1)} async-done(((bf16[3,128,256]{1,2,0:T(8,128)(2,1)}), bf16[3,2048,256]{1,2,0:T(8,128)(2,1)}) %all-gather.5.cloned.1.call-update) | async-done | bytes 3145744 | tf_op jit(solution)/shard_map/all_gather | solution.py:140
  194.9 4.6 %copy.51 = bf16[3,2048,256]{2,1,0:T(8,128)(2,1)} copy(bf16[3,2048,256]{1,2,0:T(8,128)(2,1)} %all-gather.5.cloned.1.call-done) | data formatting | bytes 6291456
  (16 shorter events, 0.3 us)
Async XLA Ops:
  7.2 58.1 %all-gather.3.cloned.1.call-start = ((), (), s32[]{:S(2)}) async-start(), calls=%async_computation.4 | async-start | bytes 3342336 | tf_op jit(solution)/shard_map/all_gather | solution.py:118
  10.7 28.9 %all-to-all-start = ((f32[16,1,16]{2,1,0:T(1,128)}), f32[16,1,16]{2,1,0:T(1,128)S(1)}, u32[]{:S(2)}, u32[]{:S(2)}) async-start(f32[16,1,16]{2,1,0:T(1,128)} %broadcast_in_dim.22), calls=%async_computation | async-start | bytes 16384 | tf_op jit(solution)/shard_map/all_to_all | solution.py:19
  19.4 20.4 %collective-permute-start = (f32[16,1]{1,0:T(8,128)S(1)}, f32[16,1]{1,0:T(8,128)S(1)}, u32[]{:S(2)}, u32[]{:S(2)}) collective-permute-start(f32[16,1]{1,0:T(8,128)S(1)} %slice.65), channel_id=1, source_target_pairs={{0,8},{8,16},{16,24},{24,32},{32,40},{40,48},{48,56},{56,64},{64,7... | collective-permute-start | bytes 200 | tf_op jit(solution)/shard_map/ppermute | solution.py:14
  91.5 25.7 %copy-start.3 = (f32[3,128,256]{2,1,0:T(8,128)S(1)}, f32[3,128,256]{2,1,0:T(8,128)}, u32[]{:S(2)}) copy-start(f32[3,128,256]{2,1,0:T(8,128)} %param.15) | copy-start | bytes 1179652
  113.2 31.3 %copy-start.2 = (bf16[3,128,256]{2,1,0:T(8,128)(2,1)S(1)}, bf16[3,128,256]{2,1,0:T(8,128)(2,1)}, u32[]{:S(2)}) copy-start(bf16[3,128,256]{2,1,0:T(8,128)(2,1)} %param.16) | copy-start | bytes 589828
  113.2 17.3 %all-to-all-start.2 = ((f32[16,1,14336]{2,1,0:T(1,128)}), f32[16,1,14336]{2,1,0:T(1,128)S(1)}, u32[]{:S(2)}, u32[]{:S(2)}) async-start(f32[16,1,14336]{2,1,0:T(1,128)} %broadcast_in_dim.24), calls=%async_computation.2 | async-start | bytes 1835008 | tf_op jit(solution)/shard_map/all_to_all | solution.py:19
  117.0 77.9 %all-gather.5.cloned.1.call-start = ((), (), s32[]{:S(2)}) async-start(), calls=%async_computation.5 | async-start | bytes 3342336 | tf_op jit(solution)/shard_map/all_gather | solution.py:140
  133.1 14.1 %copy-start.1 = (f32[3,256,256]{2,1,0:T(8,128)}, f32[3,256,256]{2,1,0:T(8,128)S(1)}, u32[]{:S(2)}) copy-start(f32[3,256,256]{2,1,0:T(8,128)S(1)} %get-tuple-element.62) | copy-start | bytes 2359300
  133.1 21.0 %copy-start = (f32[3,256,256]{2,1,0:T(8,128)}, f32[3,256,256]{2,1,0:T(8,128)S(1)}, u32[]{:S(2)}) copy-start(f32[3,256,256]{2,1,0:T(8,128)S(1)} %get-tuple-element.61) | copy-start | bytes 2359300
  133.1 16.5 %copy-start.4 = (f32[16,2048]{1,0:T(8,128)S(1)}, f32[16,2048]{1,0:T(8,128)}, u32[]{:S(2)}) copy-start(f32[16,2048]{1,0:T(8,128)} %param.19) | copy-start | bytes 393220
  133.1 16.5 %copy-start.5 = (f32[16,2048]{1,0:T(8,128)S(1)}, f32[16,2048]{1,0:T(8,128)}, u32[]{:S(2)}) copy-start(f32[16,2048]{1,0:T(8,128)} %param.20) | copy-start | bytes 393220
Sparse Core Ops, SparseCore 0:
  10.7 54.5 all-gather.2
  147.3 47.5 all-gather.4
where the time goes:
time: 208 us; the launch traced here: 206 us
  waiting for transfers between devices  72 us (35%)
  matrix products  35.5 us (17%)
  blocking collectives  28.6 us (14%)
  local copies, waits for them, and re-layouts  26.1 us (13%)
  starting transfers between devices  15.8 us (8%)
  between operations  14.9 us (7%)
  other arithmetic  13.5 us (6%)
    all_gather x1, waiting for transfers between devices, local(): lax.all_gather(proj_new.astype(jnp.bfloat16), 'fs', axis=1, tiled=True)  40.8 us
    all_to_all x1, blocking collectives, summed_on_arrival(): lax.all_to_all(parts, axis, split_axis=0, concat_axis=0, tiled=True)  19.2 us
    all_gather x1, waiting for transfers between devices, local(): all_factors = lax.all_gather(factors, 'fs', axis=1, tiled=True)  18.7 us
    dot_general x1, matrix products, local(): jnp.einsum('td,rdk->rtk', saved_input, all_factors, preferred_element_typ...  16.1 us
    all_to_all x2, waiting for transfers between devices, from_everyone(): return lax.all_to_all(copies, axis, split_axis=0, concat_axis=0, tiled=True)  12.4 us
    all_to_all x2, starting transfers between devices, from_everyone(): return lax.all_to_all(copies, axis, split_axis=0, concat_axis=0, tiled=True)  11.8 us
    unnamed x21, local copies, waits for them, and re-layouts  10.7 us
    all_to_all x1, blocking collectives, from_everyone(): return lax.all_to_all(copies, axis, split_axis=0, concat_axis=0, tiled=True)  9.37 us
  transfers between devices with their start and end apart: 5, of which 3 were waited for; matrix products, arithmetic and copies ran while one was open for 16% of the time, Pallas kernels for 0%

commit v1 on v0

--- a/solution.py
+++ b/solution.py
@@ -115,7 +115,10 @@
     later = jnp.flip(jnp.cumsum(jnp.flip(cache_cot, 1), axis=1), 1) + carried[:, None]
     gate_cot = (later * -jnp.expm1(gate_logarithm)).astype(jnp.bfloat16)
     gate_part = jnp.dot(gate_cot, saved_input, preferred_element_type=jnp.float32)
-    all_factors = lax.all_gather(factors, "fs", axis=1, tiled=True)
+    size = lax.axis_size("fs")
+    tiles = jnp.stack([factors for _ in range(size)])
+    tiles = lax.all_to_all(tiles, "fs", split_axis=0, concat_axis=0)
+    all_factors = jnp.concatenate(tiles, axis=1)
     reduced = jnp.einsum(
         "td,rdk->rtk", saved_input, all_factors, preferred_element_type=jnp.float32
     )

time: 208 us -> 222 us (1.067)
  local copies, waits for them, and re-layouts: 26.1 us -> 36.3 us
  waiting for transfers between devices: 72 us -> 63 us
  blocking collectives: 28.6 us -> 33.5 us
  other arithmetic: 13.5 us -> 17.7 us
  starting transfers between devices: 15.8 us -> 20 us
    all_gather x1 -> x0, waiting for transfers between devices: 18.7 us -> none  [local(): all_factors = lax.all_gather(factors, 'fs', axis=1, tiled=True)]
    rev x1, local copies, waits for them, and re-layouts: 1.75 us -> 9.32 us  [local(): jnp.flip(jnp.cumsum(jnp.flip(cache_cot, 1), axis=1), 1) + carried[:, None]]
    all_to_all x2, waiting for transfers between devices: 12.4 us -> 18.6 us  [from_everyone(): return lax.all_to_all(copies, axis, split_axis=0, concat_axis=0, tiled=True)]
    all_to_all x1, blocking collectives: 19.2 us -> 23.9 us  [summed_on_arrival(): lax.all_to_all(parts, axis, split_axis=0, concat_axis=0, tiled=True)]
    all_to_all x0 -> x1, starting transfers between devices: none -> 3.74 us  [local(): tiles = lax.all_to_all(tiles, 'fs', split_axis=0, concat_axis=0)]
    another operation x3, other arithmetic: 4.9 us -> 8.48 us
    ppermute x1, waiting for transfers between devices: 0.01 us -> 3.5 us  [from_behind(): return lax.ppermute(x, axis, pairs)]
    another operation x0 -> x1, local copies, waits for them, and re-layouts: none -> 2.41 us  [local(): tiles = jnp.stack([factors for _ in range(size)])]
  transfers between devices with their start and end apart: 5 -> 5, of which waited for: 3 -> 4; matrix products, arithmetic and copies ran while one was open for 16% -> 21% of each run, Pallas kernels for 0% -> 0%
where the time goes in v1:
time: 222 us; the launch traced here: 220 us
  waiting for transfers between devices  63 us (28%)
  local copies, waits for them, and re-layouts  36.3 us (16%)
  matrix products  34.7 us (16%)
  blocking collectives  33.5 us (15%)
  starting transfers between devices  20 us (9%)
  other arithmetic  17.7 us (8%)
  between operations  14.9 us (7%)
    all_gather x1, waiting for transfers between devices, local(): lax.all_gather(proj_new.astype(jnp.bfloat16), 'fs', axis=1, tiled=True)  40.8 us
    all_to_all x1, blocking collectives, summed_on_arrival(): lax.all_to_all(parts, axis, split_axis=0, concat_axis=0, tiled=True)  23.9 us
    all_to_all x2, waiting for transfers between devices, from_everyone(): return lax.all_to_all(copies, axis, split_axis=0, concat_axis=0, tiled=True)  18.6 us
    dot_general x1, matrix products, local(): jnp.einsum('td,rdk->rtk', saved_input, all_factors, preferred_element_typ...  15.2 us
    unnamed x27, local copies, waits for them, and re-layouts  12.3 us
    all_to_all x2, starting transfers between devices, from_everyone(): return lax.all_to_all(copies, axis, split_axis=0, concat_axis=0, tiled=True)  11.9 us
    all_to_all x1, blocking collectives, from_everyone(): return lax.all_to_all(copies, axis, split_axis=0, concat_axis=0, tiled=True)  9.57 us
    rev x1, local copies, waits for them, and re-layouts, local(): jnp.flip(jnp.cumsum(jnp.flip(cache_cot, 1), axis=1), 1) + carried[:, None]  9.32 us
  transfers between devices with their start and end apart: 5, of which 4 were waited for; matrix products, arithmetic and copies ran while one was open for 21% of the time, Pallas kernels for 0%

profile of v1, /device:TPU:0, one launch (start us, length us, event | category | flops | bytes accessed | tf_op | source)
XLA Modules:
  0.0 220.1 jit_solution(15955152238033543435)
XLA Ops:
  7.2 1.1 reduce_sum.36
  8.2 0.6 broadcast_in_dim.22
  8.8 8.0 %all-to-all-start.1 = ((f32[16,1,16]{2,1,0:T(1,128)}), f32[16,1,16]{2,1,0:T(1,128)S(1)}, u32[]{:S(2)}, u32[]{:S(2)}) async-start(f32[16,1,16]{2,1,0:T(1,128)} %broadcast_in_dim.22), calls=%async_computation.1 | async-start | bytes 16384 | tf_op jit(solution)/shard_map/all_to_all | solution.py:19
  16.8 1.1 copy.46
  17.9 0.0 copy-start.2
  18.0 0.0 copy-start.3
  18.0 6.4 %all-to-all-done.1 = f32[16,1,16]{2,1,0:T(1,128)S(1)} async-done(((f32[16,1,16]{2,1,0:T(1,128)}), f32[16,1,16]{2,1,0:T(1,128)S(1)}, u32[]{:S(2)}, u32[]{:S(2)}) %all-to-all-start.1) | async-done | bytes 1056 | tf_op jit(solution)/shard_map/all_to_all | solution.py:19
  24.4 0.0 copy-start.8
  24.4 2.4 %stack.2 = bf16[16,3,128,256]{2,3,1,0:T(8,128)(2,1)} broadcast(bf16[3,128,256]{1,2,0:T(8,128)(2,1)S(1)} %copy.46), dimensions={1,2,3} | broadcast | bytes 3342336 | tf_op jit(solution)/shard_map/stack | solution.py:119
  26.8 0.0 copy-done.8
  26.8 3.7 %all-to-all-start = ((bf16[16,3,128,256]{2,3,1,0:T(8,128)(2,1)}), bf16[16,3,128,256]{2,3,1,0:T(8,128)(2,1)S(1)}, u32[]{:S(2)}, u32[]{:S(2)}) async-start(bf16[16,3,128,256]{2,3,1,0:T(8,128)(2,1)} %stack.2), calls=%async_computation | async-start | bytes 6291456 | tf_op jit(solution)/shard_map/all_to_all | solution.py:120
  30.5 0.0 copy-done.2
  30.5 0.7 slice.65
  31.2 4.3 %collective-permute-start = (f32[16,1]{1,0:T(8,128)}, f32[16,1]{1,0:T(8,128)}, u32[]{:S(2)}, u32[]{:S(2)}) collective-permute-start(f32[16,1]{1,0:T(8,128)} %slice.65), channel_id=1, source_target_pairs={{0,8},{8,16},{16,24},{24,32},{32,40},{40,48},{48,56},{56,64},{64,7... | collective-permute-start | bytes 200 | tf_op jit(solution)/shard_map/ppermute | solution.py:14
  35.5 0.0 copy-done.3
  35.5 8.1 %rev.8 = f32[16,3072]{1,0:T(8,128)} reverse(f32[16,3072]{1,0:T(8,128)S(1)} %copy-done.3), dimensions={1} | reverse | bytes 393216 | tf_op jit(solution)/shard_map/jit(_flip)/rev | solution.py:115
  43.6 1.6 copy.60
  45.2 8.2 %reduce-window.6 = f32[16,24,128]{2,1,0:T(8,128)S(1)} reduce-window(f32[16,24,128]{2,1,0:T(8,128)} %bitcast.55, f32[]{:T(128)} %constant.11.clone.1), window={size=1x1x128 pad=0_0x0_0x127_0}, to_apply=%region_0.0 | reduce-window | flops 6242304 | bytes 393220 | tf_op jit(solution)/shard_map/reduce-window
  53.4 0.2 slice_reduce_fusion
  53.7 0.2 reduce-window.9
  53.8 0.1 broadcast_add_fusion
  54.0 0.7 copy.70
  54.7 9.3 %rev.9 = f32[16,3072]{1,0:T(8,128)S(1)} reverse(f32[16,3072]{1,0:T(8,128)} %bitcast.56), dimensions={1} | reverse | bytes 393216 | tf_op jit(solution)/shard_map/jit(_flip)/rev | solution.py:115
  64.0 0.8 broadcast_select_fusion
  65.0 3.5 %collective-permute-done = f32[16,1]{1,0:T(8,128)} collective-permute-done((f32[16,1]{1,0:T(8,128)}, f32[16,1]{1,0:T(8,128)}, u32[]{:S(2)}, u32[]{:S(2)}) %collective-permute-start) | collective-permute-done | bytes 96 | tf_op jit(solution)/shard_map/ppermute | solution.py:14
  68.5 6.4 %convolution_bitcast_fusion = f32[2,16,8,128]{3,2,1,0:T(8,128)S(1)} fusion(bf16[3072,2048]{1,0:T(8,128)(2,1)} %param.11, f32[16,3072]{1,0:T(8,128)S(1)} %copy-done.2, f32[16,3071]{1,0:T(8,128)S(1)} %bitcast.52, f32[16,1]{1,0:T(8,128)} %collective-permute-done, f32[16,3072]{1,0:T(8,128)S(1)} %rev.9, f32[16]{0:T(128)S(1)} %add_bitcast_fusion), kind=kOutput, calls=%fused_computation.12 | convolution fusion | flops 201621504 | bytes 13303872 | tf_op jit(solution)/shard_map/dot_general | solution.py:117
  74.9 0.0 all-to-all-done
  74.9 15.2 %bitcast_convert_fusion = (bf16[3,3072,256]{1,2,0:T(8,128)(2,1)S(1)}, f32[3,256,3072]{2,1,0:T(8,128)}) fusion(bf16[3072,2048]{1,0:T(8,128)(2,1)} %param.11, bf16[16,3,128,256]{2,3,1,0:T(8,128)(2,1)S(1)} %all-to-all-done), kind=kOutput, calls=%fused_computation.3 | convolution fusion | flops 9666035712 | bytes 29884416 | tf_op jit(solution)/shard_map/td,rdk->rtk/dot_general | solution.py:122
  90.1 3.8 %fusion.24 = f32[3,256,256]{2,1,0:T(8,128)S(1)} fusion(bf16[3,3072,256]{1,2,0:T(8,128)(2,1)S(1)} %get-tuple-element.63, bf16[3,3072,256]{2,1,0:T(8,128)(2,1)} %param.12), kind=kOutput, calls=%fused_computation.38 | convolution fusion | flops 1207959552 | bytes 10223616 | tf_op jit(solution)/shard_map/rtk,rtw->rkw/dot_general | solution.py:127
  93.8 6.7 %fusion.7 = f32[3,256,256]{2,1,0:T(8,128)S(1)} fusion(f32[3,256,256]{2,1,0:T(8,128)S(1)} %fusion.24, bf16[3,3072,256]{2,1,0:T(8,128)(2,1)} %param.12, f32[3,256,3072]{2,1,0:T(8,128)} %get-tuple-element.64, bf16[3,3072,256]{1,2,0:T(8,128)(2,1)S(1)} %get-tuple-element.63), kind=kOutput, calls=%fused_computation.8 | convolution fusion | flops 1215234048 | bytes 20447232 | tf_op jit(solution)/shard_map/rtk,rtw->rkw/dot_general | solution.py:128
  100.5 0.0 copy-start.5
  100.5 0.4 copy.59
  100.9 0.1 pad_maximum_fusion
  101.0 23.9 %all_to_all.35 = f32[16,1,14336]{2,1,0:T(1,128)S(1)} all-to-all(f32[16,1,14336]{2,1,0:T(1,128)S(1)} %bitcast.49), channel_id=1, replica_groups=mesh['fs'=16,'tp'=8] {'fs'}, dimensions={0} | all-to-all | bytes 1835008 | tf_op jit(solution)/shard_map/all_to_all | solution.py:67
  124.9 0.6 reduce_sum.37
  125.5 1.4 broadcast_in_dim.24
  126.9 0.0 copy-start.4
  126.9 3.9 %all-to-all-start.3 = ((f32[16,1,14336]{2,1,0:T(1,128)}), f32[16,1,14336]{2,1,0:T(1,128)S(1)}, u32[]{:S(2)}, u32[]{:S(2)}) async-start(f32[16,1,14336]{2,1,0:T(1,128)} %broadcast_in_dim.24), calls=%async_computation.3 | async-start | bytes 1835008 | tf_op jit(solution)/shard_map/all_to_all | solution.py:19
  130.9 0.0 all-gather.2.cloned.1.call-start
  130.9 0.0 copy-done.5
  130.9 0.9 copy.51
  131.8 12.2 %all-to-all-done.3 = f32[16,1,14336]{2,1,0:T(1,128)S(1)} async-done(((f32[16,1,14336]{2,1,0:T(1,128)}), f32[16,1,14336]{2,1,0:T(1,128)S(1)}, u32[]{:S(2)}, u32[]{:S(2)}) %all-to-all-start.3) | async-done | bytes 917536 | tf_op jit(solution)/shard_map/all_to_all | solution.py:19
  144.1 0.1 slice.72
  144.1 0.2 reshape.79
  144.4 2.3 %multiply_reduce_fusion = (f32[]{:T(128)}, f32[3,256,256]{2,1,0:T(8,128)S(1)}, f32[3,256,256]{2,1,0:T(8,128)S(1)}) fusion(f32[3,256,256]{2,1,0:T(8,128)S(1)} %reshape.79, f32[3,256,256]{2,1,0:T(8,128)} %param.18, f32[3,256,256]{2,1,0:T(8,128)} %param.17), kind=kLoop, calls=%fused_computation.15 | loop fusion | flops 1966079 | bytes 3932164 | tf_op jit(solution)/shard_map/reduce_sum | solution.py:135
  146.6 0.0 copy-start.1
  146.6 0.0 copy-start
  146.6 0.7 broadcast_in_dim.25
  147.4 9.6 %all_to_all.36 = f32[8,1,1]{2,1,0:T(1,128)S(1)} all-to-all(f32[8,1,1]{2,1,0:T(1,128)S(1)} %broadcast_in_dim.25), channel_id=1, replica_groups=mesh['fs'=16,'tp'=8] {'tp'}, dimensions={0} | all-to-all | bytes 64 | tf_op jit(solution)/shard_map/all_to_all | solution.py:19
  156.9 0.6 reduce_sum.39
  158.2 0.0 copy-done.4
  158.3 2.7 %fusion.22 = (bf16[3,128,256]{1,2,0:T(8,128)(2,1)}, f32[3,128,256]{1,2,0:T(8,128)S(1)}, f32[3,128,256]{1,2,0:T(8,128)}) fusion(f32[3,128,256]{1,2,0:T(8,128)} %copy.51, bf16[3,128,256]{2,1,0:T(8,128)(2,1)S(1)} %copy-done.4, f32[3,256,256]{2,1,0:T(8,128)S(1)} %get-tuple-element.62, f32[3,256,256]{2,1,0:T(8,128)S(1)} %get-tuple-element.61, f32[]{:T(128)S(6)} %rsqrt.5), kind=kOutput, calls=%fused_computation.37 | convolution fusion | flops 302579712 | bytes 3145732 | tf_op jit(solution)/shard_map/rdk,rkw->rdw/dot_general | solution.py:138
  160.9 0.0 copy-done.1
  160.9 0.0 all-gather.2.cloned.1.call-update
  160.9 2.2 reduce.3
  163.1 0.1 slice.68
  163.3 0.0 copy-done.6
  163.3 0.0 copy-done.7
  163.3 1.7 fusion.20
  165.0 1.9 copy.52
  166.9 0.9 copy.53
  167.8 0.0 copy-done
  167.8 40.8 %all-gather.2.cloned.1.call-done = bf16[3,2048,256]{1,2,0:T(8,128)(2,1)} async-done(((bf16[3,128,256]{1,2,0:T(8,128)(2,1)}), bf16[3,2048,256]{1,2,0:T(8,128)(2,1)}) %all-gather.2.cloned.1.call-update) | async-done | bytes 3145744 | tf_op jit(solution)/shard_map/all_gather | solution.py:143
  208.7 4.6 %copy.54 = bf16[3,2048,256]{2,1,0:T(8,128)(2,1)} copy(bf16[3,2048,256]{1,2,0:T(8,128)(2,1)} %all-gather.2.cloned.1.call-done) | data formatting | bytes 6291456
  (16 shorter events, 0.2 us)
Async XLA Ops:
  8.8 15.5 %all-to-all-start.1 = ((f32[16,1,16]{2,1,0:T(1,128)}), f32[16,1,16]{2,1,0:T(1,128)S(1)}, u32[]{:S(2)}, u32[]{:S(2)}) async-start(f32[16,1,16]{2,1,0:T(1,128)} %broadcast_in_dim.22), calls=%async_computation.1 | async-start | bytes 16384 | tf_op jit(solution)/shard_map/all_to_all | solution.py:19
  17.9 12.6 %copy-start.2 = (f32[16,3072]{1,0:T(8,128)S(1)}, f32[16,3072]{1,0:T(8,128)}, u32[]{:S(2)}) copy-start(f32[16,3072]{1,0:T(8,128)} %param.13) | copy-start | bytes 589828
  18.0 17.5 %copy-start.3 = (f32[16,3072]{1,0:T(8,128)S(1)}, f32[16,3072]{1,0:T(8,128)}, u32[]{:S(2)}) copy-start(f32[16,3072]{1,0:T(8,128)} %param.14) | copy-start | bytes 589828
  24.4 2.4 %copy-start.8 = (f32[16,1,16]{2,1,0:T(1,128)}, f32[16,1,16]{2,1,0:T(1,128)S(1)}, u32[]{:S(2)}) copy-start(f32[16,1,16]{2,1,0:T(1,128)S(1)} %all-to-all-done.1) | copy-start | bytes 3076
  26.8 48.1 %all-to-all-start = ((bf16[16,3,128,256]{2,3,1,0:T(8,128)(2,1)}), bf16[16,3,128,256]{2,3,1,0:T(8,128)(2,1)S(1)}, u32[]{:S(2)}, u32[]{:S(2)}) async-start(bf16[16,3,128,256]{2,3,1,0:T(8,128)(2,1)} %stack.2), calls=%async_computation | async-start | bytes 6291456 | tf_op jit(solution)/shard_map/all_to_all | solution.py:120
  31.2 37.3 %collective-permute-start = (f32[16,1]{1,0:T(8,128)}, f32[16,1]{1,0:T(8,128)}, u32[]{:S(2)}, u32[]{:S(2)}) collective-permute-start(f32[16,1]{1,0:T(8,128)} %slice.65), channel_id=1, source_target_pairs={{0,8},{8,16},{16,24},{24,32},{32,40},{40,48},{48,56},{56,64},{64,7... | collective-permute-start | bytes 200 | tf_op jit(solution)/shard_map/ppermute | solution.py:14
  100.5 30.4 %copy-start.5 = (f32[3,128,256]{2,1,0:T(8,128)S(1)}, f32[3,128,256]{2,1,0:T(8,128)}, u32[]{:S(2)}) copy-start(f32[3,128,256]{2,1,0:T(8,128)} %param.15) | copy-start | bytes 1179652
  126.9 31.3 %copy-start.4 = (bf16[3,128,256]{2,1,0:T(8,128)(2,1)S(1)}, bf16[3,128,256]{2,1,0:T(8,128)(2,1)}, u32[]{:S(2)}) copy-start(bf16[3,128,256]{2,1,0:T(8,128)(2,1)} %param.16) | copy-start | bytes 589828
  126.9 17.2 %all-to-all-start.3 = ((f32[16,1,14336]{2,1,0:T(1,128)}), f32[16,1,14336]{2,1,0:T(1,128)S(1)}, u32[]{:S(2)}, u32[]{:S(2)}) async-start(f32[16,1,14336]{2,1,0:T(1,128)} %broadcast_in_dim.24), calls=%async_computation.3 | async-start | bytes 1835008 | tf_op jit(solution)/shard_map/all_to_all | solution.py:19
  130.9 77.8 %all-gather.2.cloned.1.call-start = ((), (), s32[]{:S(2)}) async-start(), calls=%async_computation.5 | async-start | bytes 3342336 | tf_op jit(solution)/shard_map/all_gather | solution.py:143
  146.6 14.3 %copy-start.1 = (f32[3,256,256]{2,1,0:T(8,128)}, f32[3,256,256]{2,1,0:T(8,128)S(1)}, u32[]{:S(2)}) copy-start(f32[3,256,256]{2,1,0:T(8,128)S(1)} %get-tuple-element.62) | copy-start | bytes 2359300
  146.6 21.2 %copy-start = (f32[3,256,256]{2,1,0:T(8,128)}, f32[3,256,256]{2,1,0:T(8,128)S(1)}, u32[]{:S(2)}) copy-start(f32[3,256,256]{2,1,0:T(8,128)S(1)} %get-tuple-element.61) | copy-start | bytes 2359300
  146.6 16.7 %copy-start.6 = (f32[16,2048]{1,0:T(8,128)S(1)}, f32[16,2048]{1,0:T(8,128)}, u32[]{:S(2)}) copy-start(f32[16,2048]{1,0:T(8,128)} %param.19) | copy-start | bytes 393220
  146.6 16.7 %copy-start.7 = (f32[16,2048]{1,0:T(8,128)S(1)}, f32[16,2048]{1,0:T(8,128)}, u32[]{:S(2)}) copy-start(f32[16,2048]{1,0:T(8,128)} %param.20) | copy-start | bytes 393220
Sparse Core Ops, SparseCore 0:
  161.1 47.5 all-gather.1
